TPU v7x, 256 devices: a whole 4x4x8 slice. The times are simulated.
256 devices in a mesh: ep: 64 (over z, x, core), tp: 4 (over y).
Axes of the slice: x: 4, y: 4, z: 8, core: 2. Of those that a mesh axis runs over, the one named last changes fastest.
Arguments:
- receptance: bfloat16 [32768, 2048], P('ep', 'tp'), may hold values from -6 to 6
- key_rows: bfloat16 [32768, 2048], P('ep', 'tp'), may hold values from -6 to 6
- value_rows: bfloat16 [32768, 2048], P('ep', 'tp'), may hold values from -6 to 6
- decay_input: bfloat16 [32768, 2048], P('ep', 'tp'), may hold values from -2.796875 to 2.796875
- learn_input: bfloat16 [32768, 2048], P('ep', 'tp'), may hold values from -12 to 4
- decay_base: float32 [2048], P('tp'), may hold values from -20 to -2
- decay_shift: float32 [32768, 32], P('ep', 'tp'), may hold values from -1 to 20
- channel_gain: float32 [2048], P('tp'), may hold values from 0.1 to 1.9
- out_weight: bfloat16 [2048, 2048], P('tp'), may hold values from -0.125 to 0.125
- expert_input: bfloat16 [32768, 2048], P(('ep', 'tp')), may hold values from -6 to 6
- expert_gain: float32 [2048], replicated, may hold values from 0.1 to 1.9
- routes: int32 [32768, 2], P(('ep', 'tp')), may hold values from 0 to 63, all different within a row; in each aligned block of 128 rows (0 to 127, 128 to 255, ...) at most 8 rows name the same one
- route_weight: float32 [32768, 2], P(('ep', 'tp')), may hold values from 0.1 to 1
- gate_weight: bfloat16 [64, 2048, 1024], P('ep', None, 'tp'), may hold values from -0.125 to 0.125
- up_weight: bfloat16 [64, 2048, 1024], P('ep', None, 'tp'), may hold values from -0.125 to 0.125
- down_weight: bfloat16 [64, 1024, 2048], P('ep', 'tp'), may hold values from -0.1875 to 0.1875
Outputs:
- mixer_out: bfloat16 [32768, 2048], P(('ep', 'tp'))
- expert_out: bfloat16 [32768, 2048], P(('ep', 'tp'))
Inputs may be any that keep to these rules, and one draw needn't show every extreme that they name: `routes`: within the rows of one device (aligned blocks of 128 rows) no expert is named by more than 8 rows, and in every draw some block names some expert exactly 8 times. Each row names 2 different experts.
All inputs are finite; a program needn't handle non-finite values.
Results may differ from a plain program's by a relative error of at most 0.024.
Values may be sent and summed in bfloat16 or wider, within the bound.
A program may use at most 128 MiB of HBM per device.

v0:
```python
import functools

import jax
import jax.numpy as jnp
from jax import lax
from jax.experimental import pallas as pl
from jax.experimental.pallas import tpu as pltpu
from jax.sharding import PartitionSpec as P


MESH = pl.DeviceIdType.MESH
NORM_EPS = 1e-06
GROUP_EPS = 0.00064
F=jnp.float32; B=jnp.bfloat16
C=64
NT=(((1,),(1,)),((),())); NN=(((1,),(0,)),((),())); TN=(((0,),(0,)),((),()))
def dg(a,b,dims): return lax.dot_general(a,b,dims,preferred_element_type=F)
def split(x):
    hi=x.astype(B); return hi,(x-hi.astype(F)).astype(B)
def dot3(a,b,dims):
    ah,al=split(a); bh,bl=split(b)
    return dg(ah,bh,dims)+(dg(ah,bl,dims)+dg(al,bh,dims))
def fold(x,n): return x[:n]+x[n:]
def consts():
    r=lax.broadcasted_iota(jnp.int32,(128,128),0); c=lax.broadcasted_iota(jnp.int32,(128,128),1)
    same=(r//64)==(c//64)
    return r,c,same
def pre_stage(key,dec,learn,base,s0,s1):
    r,c,same=consts()
    ones=same.astype(B)
    kf=key.astype(F)
    hi,lo=split(kf*kf)
    ss=dg(hi,ones,NN)+dg(lo,ones,NN)
    unit=kf*lax.rsqrt(ss+1e-6)
    lane=lax.broadcasted_iota(jnp.int32,key.shape,1)
    pre=dec.astype(F)+base+jnp.where(lane<64,s0,s1)
    ld=-0.6065306597126334/(1.0+jnp.exp(-pre))
    rem=unit/(1.0+jnp.exp(-learn.astype(F)))
    return kf,unit,ld,rem
def chunk_cum(ld):
    r,c,same=consts()
    tri=(same&(r>=c)).astype(B)
    outs=[]
    for i in range(ld.shape[0]//128):
        hi,lo=split(ld[i*128:(i+1)*128])
        outs.append(dg(tri,hi,NN)+dg(tri,lo,NN))
    return jnp.concatenate(outs,0)
def chunk(rec,kf,vb,unit,rem,ld,cum):
    r,c,same=consts()
    lane=lax.broadcasted_iota(jnp.int32,(C,128),1)
    m0=lane<64
    mid=cum[C//2-1:C//2]; end=cum[C-1:C]
    rel=cum-mid
    Q=rec*jnp.exp(rel); P=unit*jnp.exp(rel-ld)
    sh=jnp.exp(-rel)
    BR=(rem*sh).astype(B); BK=(kf*sh).astype(B)
    Qb=Q.astype(B); Pb=P.astype(B)
    z=jnp.zeros((C,128),B)
    ex=lambda x: jnp.concatenate([jnp.where(m0,x,z),jnp.where(m0,z,x)],0)
    Pe=ex(Pb)
    lhs=jnp.concatenate([Pe,ex(Qb)],0)
    sR=dg(lhs,jnp.concatenate([BR,BR],0),NT)
    sK=dg(lhs,jnp.concatenate([BK,BK],0),NT)
    yield None
    strict=same&(r>c); incl=same&(r>=c)
    zf=jnp.zeros((128,128),F)
    A=jnp.where(strict,sR[:128],zf).astype(B)
    PK=jnp.where(strict,sK[:128],zf).astype(B)
    QR=jnp.where(incl,sR[128:],zf).astype(B)
    QK=jnp.where(incl,sK[128:],zf).astype(B)
    zb=jnp.zeros((128,128),B)
    x=r^c
    lm=lambda m: (x>=m)&(x<2*m)
    D=jnp.where(r==c,1.0,0.0).astype(B)-jnp.where(lm(1),A,zb)
    m=2
    while m<C:
        E=dg(jnp.where(lm(m),A,zb),D,NN).astype(B)
        yield None
        D=D-dg(D,E,NN).astype(B)
        yield None
        m*=2
    Ve=ex(vb)
    kv=dg(jnp.concatenate([PK,QK],0),Ve,NN)
    yield None
    X=dg(D,jnp.concatenate([Pe,kv[:128].astype(B)],1),NN)
    Xb=X.astype(B)
    yield None
    qx=dg(QR,Xb,NN)
    yield None
    em=jnp.exp(mid); et=jnp.exp(end-mid)
    reader=(Q-fold(qx[:,:128],C))*em
    local=fold(kv[128:],C)-fold(qx[:,128:],C)
    X0=fold(Xb[:,:128],C); L=fold(Xb[:,128:],C)
    tx=dg(X0,BR,TN)
    yield None
    eye=jnp.where(r==c,1.0,0.0).astype(F)
    emT=jnp.sum(jnp.where(r==c,jnp.broadcast_to(em,(128,128)),zf),1,keepdims=True)
    T=jnp.where(same,(eye-tx)*emT*et,zf)
    off=dg(jnp.concatenate([vb,-L],0),jnp.concatenate([BK,BR],0),TN)
    off=jnp.where(same,off*et,zf)
    yield reader,local,T,off
def local_scan(rec,key,val,dec,learn,base,s0,s1):
    n=key.shape[0]//C
    kf,unit,ld,rem=pre_stage(key,dec,learn,base,s0,s1)
    cum=chunk_cum(ld)
    outs=[]
    for i in range(n):
        s=slice(i*C,(i+1)*C)
        outs.append(chunk(rec[s].astype(F),kf[s],val[s],unit[s],rem[s],ld[s],cum[s]))
    while True:
        now=[next(o) for o in outs]
        if now[0] is not None: break
    outs=now
    r,c,same=consts()
    PB=None
    rd=[];lc=[]
    for i in range(n):
        reader,local,T,off=outs[i]
        if PB is None:
            rd.append(reader); lc.append(local)
            PB=jnp.concatenate([T,off],0)
        else:
            ph,pl_=split(PB)
            rh=reader.astype(B)
            q=dg(rh,ph,NT)
            rd.append(q[:,:128]); lc.append(local+q[:,128:])
            PB=dot3(PB,T,NN)+jnp.concatenate([jnp.zeros_like(off),off],0)
    return jnp.concatenate(rd,0),jnp.concatenate(lc,0),PB[:128],PB[128:]


def spread(compact):
    lane = lax.broadcasted_iota(jnp.int32, compact.shape, 1)
    nil = jnp.zeros_like(compact)
    return jnp.concatenate([jnp.where(lane < 64, compact, nil), jnp.where(lane < 64, nil, compact)], 0)


def unpack(message):
    r, c, same = consts()
    eye = jnp.where(r == c, 1.0, 0.0).astype(F)
    wide = message.astype(F)
    return spread(wide[:C]) + eye, wide[C:]


def head_sum(x, ones):
    hi, lo = split(x)
    return dg(hi, ones, NN) + dg(lo, ones, NN)


def remote(src, dst, send, recv, where):
    return pltpu.make_async_remote_copy(
        src_ref=src, dst_ref=dst, send_sem=send, recv_sem=recv, device_id=where, device_id_type=MESH
    )


def wait_bytes(ref, sem):
    pltpu.make_async_copy(ref, ref, sem).wait()


def kernel(
    rec_hbm, key_hbm, val_hbm, dec_hbm, learn_hbm, wout_hbm, x_hbm, gate_hbm, up_hbm, down_hbm,
    base_ref, shift_ref, gain_ref, xgain_ref, routes_ref, rw_ref,
    mixer_ref, expert_ref,
    mix_in, wout, xin, g_buf, u_buf, d_buf, rd_buf, lc_buf, mb_buf, row_buf, exc_buf, tz_buf, z_buf, fin_buf, st_buf,
    wt_buf, out_buf, arr_buf, acc, res_buf, ret_buf, part_buf, rs_buf,
    in_sems, own_sems, ws, wr, s1, r1, s2, r2, s3, r3, s4, r4, misc, go,
):
    ep, tp = lax.axis_index("ep"), lax.axis_index("tp")
    z, m = ep // 8, ep % 8
    x, core = m // 2, m % 2
    n = 64
    right, left = (tp + 1) % 4, (tp + 3) % 4

    loads = [pltpu.make_async_copy(x_hbm, xin, in_sems.at[0])]
    for i, src in enumerate((rec_hbm, key_hbm, val_hbm, dec_hbm, learn_hbm)):
        loads.append(pltpu.make_async_copy(src, mix_in.at[i], in_sems.at[i + 1]))
    loads.append(pltpu.make_async_copy(wout_hbm, wout, in_sems.at[6]))
    own = [
        pltpu.make_async_copy(src, dst.at[0], own_sems.at[i])
        for i, (src, dst) in enumerate(((gate_hbm, g_buf), (up_hbm, u_buf), (down_hbm, d_buf)))
    ]
    for load in loads + own:
        load.start()

    barrier = pltpu.get_barrier_semaphore()

    @pl.loop(1, n)
    def _(d):
        pl.semaphore_signal(barrier, inc=1, device_id={"ep": (ep + d) % n}, device_id_type=MESH)

    for d in range(1, 4):
        pl.semaphore_signal(barrier, inc=1, device_id={"tp": (tp + d) % 4}, device_id_type=MESH)
    pl.semaphore_wait(barrier, n - 1 + 3)

    half = d_buf.shape[1] // 2
    top, bottom = pl.ds(0, half), pl.ds(half, half)
    ahead, back = {"tp": right}, {"tp": left}
    near = [
        remote(gate_hbm, g_buf.at[1], ws.at[0], wr.at[0], ahead),
        remote(up_hbm, u_buf.at[2], ws.at[1], wr.at[1], back),
        remote(down_hbm, d_buf.at[1], ws.at[2], wr.at[2], ahead),
        remote(down_hbm, d_buf.at[2], ws.at[3], wr.at[3], back),
        remote(up_hbm, u_buf.at[1], ws.at[4], wr.at[4], ahead),
        remote(gate_hbm, g_buf.at[2], ws.at[5], wr.at[5], back),
    ]
    far = [
        remote(g_buf.at[1], g_buf.at[3], ws.at[6], wr.at[6], ahead),
        remote(u_buf.at[2], u_buf.at[3], ws.at[7], wr.at[7], back),
        remote(d_buf.at[1, top], d_buf.at[3, top], ws.at[8], wr.at[8], ahead),
        remote(d_buf.at[2, bottom], d_buf.at[3, bottom], ws.at[9], wr.at[9], back),
    ]

    def forward():
        for i in range(4):
            near[i].wait_recv()
            far[i].start()

    @pl.when(core == 0)
    def _():
        for copy in near:
            copy.start()

    loads[0].wait()
    rows = xin[...].astype(F)
    normed = (rows * lax.rsqrt(jnp.mean(rows * rows, axis=1, keepdims=True) + NORM_EPS) * xgain_ref[...]).astype(B)
    named = routes_ref[...]
    r0, r1_ = named[:, 0:1], named[:, 1:2]
    r, c, same = consts()
    hits = ((c == r0) | (c == r1_)).astype(F).astype(B)
    earlier = dg((r > c).astype(F).astype(B), hits, NN)
    t0 = r0.astype(F) * 8.0 + jnp.sum(jnp.where(c == r0, earlier, 0.0), 1, keepdims=True)
    t1 = r1_.astype(F) * 8.0 + jnp.sum(jnp.where(c == r1_, earlier, 0.0), 1, keepdims=True)
    place = lax.broadcasted_iota(jnp.int32, (128, n * 8), 1).astype(F)
    first, second = place == t0, place == t1
    marks = jnp.where(first | second, 1.0, 0.0).astype(B)
    shares = jnp.where(first, rw_ref[:, 0:1], 0.0) + jnp.where(second, rw_ref[:, 1:2], 0.0)
    hi, lo = split(shares)
    wt_buf[0] = hi
    wt_buf[1] = lo
    for b in range(4):
        out_buf[16 * b : 16 * b + 16] = (
            dg(marks[:, 128 * b : 128 * b + 128], normed, TN).reshape(16, 8, -1).astype(B)
        )

    def send_rows(src, dst, sem, there):
        remote(src.at[there], dst.at[ep], sem.at[0], sem.at[1], {"ep": there}).start()

    @pl.loop(0, n // 2)
    def _(d):
        send_rows(out_buf, arr_buf, s4, (ep + 2 * d + 1) % n)

    for load in loads[1:6]:
        load.wait()

    @pl.loop(0, 4)
    def _(p):
        lanes = pl.ds(pl.multiple_of(p * 128, 128), 128)
        shift = shift_ref[...]
        heads = lax.broadcasted_iota(jnp.int32, shift.shape, 1)
        h0 = jnp.sum(jnp.where(heads == 2 * p, shift, 0.0), 1, keepdims=True)
        h1 = jnp.sum(jnp.where(heads == 2 * p + 1, shift, 0.0), 1, keepdims=True)
        a = [mix_in[i, :, lanes] for i in range(5)]
        rd, lc, whole, offset = local_scan(*a, base_ref[:, lanes], h0, h1)
        rd_buf[:, lanes] = rd.astype(B)
        lc_buf[:, lanes] = lc
        r, c, same = consts()
        less = fold(whole - jnp.where(r == c, 1.0, 0.0), C)
        mb_buf[p] = jnp.concatenate([less, fold(offset, C)], 0).astype(B)

    def row_copy(d, slot):
        j = (m + d) % 8
        return remote(mb_buf.at[j // 2], row_buf.at[slot], s1.at[d], r1.at[slot], {"ep": z * 8 + j})

    for d in range(1, 8):
        row_copy(d, m).start()

    @pl.when(core == 0)
    def _():
        forward()

    row_buf[m] = mb_buf[x]
    for d in range(1, 8):
        row_copy(d, (m + d) % 8).wait_recv()
    eye = fold(jnp.where(r == c, 1.0, 0.0).astype(F), C)
    none = jnp.zeros((C, 128), F)
    running = jnp.concatenate([eye, none], 0)
    for j in range(8):
        exc_buf[j] = running
        step, offset = unpack(row_buf[j])
        if j == 0:
            running = jnp.concatenate([fold(step, C), offset], 0)
        else:
            running = dot3(running, step, NN) + jnp.concatenate([none, offset], 0)
    tz_buf[...] = (running - jnp.concatenate([eye, none], 0)).astype(B)

    def z_copy(d, slot):
        return remote(tz_buf, z_buf.at[slot], s2.at[d], r2.at[slot], {"ep": ((z + d) % 8) * 8 + m})

    for d in range(1, 8):
        z_copy(d, z).start()

    @pl.loop(1, n // 2)
    def _(d):
        send_rows(out_buf, arr_buf, s4, (ep + 2 * d) % n)

    arr_buf[ep] = out_buf[ep]
    z_buf[z] = tz_buf[...]
    for d in range(1, 8):
        z_copy(d, (z + d) % 8).wait_recv()
    state = none
    for j in range(7):
        step, offset = unpack(z_buf[j])
        after = offset if j == 0 else dot3(state, step, NN) + offset
        state = jnp.where(j < z, after, state)
    for k in range(4):
        member = exc_buf[k * 2 + core]
        fin_buf[k] = (dot3(state, spread(member[:C]), NN) + member[C:]).astype(B)

    def fin_copy(d, slot):
        k = (x + d) % 4
        return remote(fin_buf.at[k], st_buf.at[slot], s3.at[d], r3.at[slot], {"ep": z * 8 + k * 2 + core})

    for d in range(1, 4):
        fin_copy(d, x).start()

    @pl.when(core == 1)
    def _():
        for copy in near:
            copy.start()

    st_buf[x] = fin_buf[x]
    for d in range(1, 4):
        fin_copy(d, (x + d) % 4).wait_recv()

    loads[6].wait()
    ones = jnp.where(same, 1.0 / 64, 0.0).astype(B)
    for b in range(4):
        here = slice(128 * b, 128 * b + 128)
        parts = []
        for p in range(4):
            lanes = slice(p * 128, (p + 1) * 128)
            read = lc_buf[here, lanes] + dg(rd_buf[here, lanes], spread(st_buf[p]), NT)
            centred = read - head_sum(read, ones)
            variance = head_sum(centred * centred, ones)
            parts.append((centred * lax.rsqrt(variance + GROUP_EPS) * gain_ref[:, lanes]).astype(B))
        part_buf[b] = dg(jnp.concatenate(parts, 1), wout[...], NN).astype(B)

    wait_bytes(arr_buf.at[pl.ds(0, n - 1)], s4.at[1])
    for copy in own:
        copy.wait()

    def units(s, b):
        given = arr_buf[pl.ds(16 * b, 16)].reshape(128, -1)
        gate = dg(given, g_buf[s], NN)
        up = dg(given, u_buf[s], NN)
        hidden = (gate / (1.0 + jnp.exp(-gate)) * up).astype(B)
        return dg(hidden, d_buf[s], NN)

    def rows_of(b):
        return pl.ds(pl.multiple_of(b * 128, 128), 128)

    @pl.loop(0, 4)
    def _(b):
        acc[rows_of(b), :] = units(0, b)

    @pl.when(core == 1)
    def _():
        forward()

    near[4].wait_recv()

    @pl.loop(0, 4)
    def _(b):
        acc[rows_of(b), :] += units(1, b)

    near[5].wait_recv()

    @pl.loop(0, 4)
    def _(b):
        acc[rows_of(b), :] += units(2, b)

    for copy in far:
        copy.wait_recv()

    @pl.when(core == 1)
    def _():
        pl.semaphore_signal(go, inc=1, device_id={"ep": ep - 1}, device_id_type=MESH)

    @pl.loop(0, 4)
    def _(i):
        b = (z // 2 + i) % 4
        res_buf[pl.ds(16 * b, 16)] = (acc[rows_of(b), :] + units(3, b)).reshape(16, 8, -1).astype(B)

        @pl.loop(0, 16)
        def _(k):
            there = 16 * b + (ep + k) % 16

            @pl.when(there != ep)
            def _():
                send_rows(res_buf, ret_buf, misc, there)

    @pl.when(core == 0)
    def _():
        pl.semaphore_wait(go, 1)

    def rs_copy(d, slot):
        j = (tp + d) % 4
        return remote(part_buf.at[j], rs_buf.at[slot], ws.at[9 + d], wr.at[10 + slot], {"tp": j})

    for d in range(1, 4):
        rs_copy(d, tp).start()
    ret_buf[ep] = res_buf[ep]
    total = part_buf[tp].astype(F)
    for d in range(1, 4):
        rs_copy(d, (tp + d) % 4).wait_recv()
        total += rs_buf[(tp + d) % 4].astype(F)
    mixer_ref[...] = total.astype(B)

    wait_bytes(ret_buf.at[pl.ds(0, n - 1)], misc.at[1])
    back_rows = ret_buf[...].reshape(n * 8, -1)
    expert_ref[...] = (dg(wt_buf[0], back_rows, NN) + dg(wt_buf[1], back_rows, NN)).astype(B)

    for copy in near + far:
        copy.wait_send()
    for d in range(1, 8):
        row_copy(d, m).wait_send()
        z_copy(d, z).wait_send()
    for d in range(1, 4):
        fin_copy(d, x).wait_send()
        rs_copy(d, tp).wait_send()
    wait_bytes(out_buf.at[pl.ds(0, n - 1)], s4.at[0])
    wait_bytes(res_buf.at[pl.ds(0, n - 1)], misc.at[0])


def on_device(
    receptance, key_rows, value_rows, decay_input, learn_input, decay_base, decay_shift, channel_gain,
    out_weight, expert_input, expert_gain, routes, route_weight, gate_weight, up_weight, down_weight,
):
    t, width = expert_input.shape
    rows, channels = receptance.shape
    depth, units = gate_weight.shape[1:]
    vmem = pl.BlockSpec(memory_space=pltpu.VMEM)
    anywhere = pl.BlockSpec(memory_space=pl.ANY)
    dma = pltpu.SemaphoreType.DMA
    V = pltpu.VMEM
    return pl.pallas_call(
        kernel,
        in_specs=[anywhere] * 10 + [vmem] * 6,
        out_specs=[vmem, vmem],
        out_shape=[jax.ShapeDtypeStruct((t, width), B)] * 2,
        scratch_shapes=[
            V((5, rows, channels), B), V((channels, width), B), V((t, width), B),
            V((4, depth, units), B), V((4, depth, units), B), V((4, units, width), B),
            V((rows, channels), B), V((rows, channels), F),
            V((4, 128, 128), B), V((8, 128, 128), B), V((8, 128, 128), F), V((128, 128), B), V((8, 128, 128), B),
            V((4, C, 128), B), V((4, C, 128), B),
            V((2, t, 512), B), V((64, 8, width), B), V((64, 8, width), B), V((512, width), F),
            V((64, 8, width), B), V((64, 8, width), B), V((4, t, width), B), V((4, t, width), B),
            dma((7,)), dma((3,)), dma((13,)), dma((14,)), dma((8,)), dma((8,)), dma((8,)), dma((8,)), dma((4,)), dma((4,)),
            dma((2,)), dma((2,)), dma((2,)), pltpu.SemaphoreType.REGULAR,
        ],
        compiler_params=pltpu.CompilerParams(
            collective_id=0, has_side_effects=True, vmem_limit_bytes=60 * 1024 * 1024
        ),
        name="step",
    )(
        receptance, key_rows, value_rows, decay_input, learn_input, out_weight, expert_input,
        gate_weight[0], up_weight[0], down_weight[0],
        decay_base.reshape(1, channels), decay_shift, channel_gain.reshape(1, channels), expert_gain.reshape(1, width),
        routes, route_weight,
    )


def solution(mesh):
    both = P(("ep", "tp"), None)
    placed = (
        P("ep", "tp"), P("ep", "tp"), P("ep", "tp"), P("ep", "tp"), P("ep", "tp"), P("tp"), P("ep", "tp"), P("tp"),
        P("tp", None), both, P(), both, both, P("ep", None, "tp"), P("ep", None, "tp"), P("ep", "tp", None),
    )
    return jax.shard_map(on_device, mesh=mesh, in_specs=placed, out_specs=(both, both), check_vma=False)
```

profile of v0, /device:TPU:1, one launch (start us, length us, event | category | flops | bytes accessed | tf_op | source)
XLA Modules:
  0.0 156.3 jit_solution(17756187263766263558)
XLA Ops:
  0.6 1.4 copy.19.routes_ref
  2.0 1.4 copy.20.rw_ref
  3.5 1.6 copy.18.shift_ref
  5.0 147.5 %step.1 = (bf16[128,2048]{1,0:T(8,128)(2,1)}, bf16[128,2048]{1,0:T(8,128)(2,1)}) custom-call(bf16[512,512]{1,0:T(8,128)(2,1)} %rec_hbm.1, bf16[512,512]{1,0:T(8,128)(2,1)} %key_hbm.1, bf16[512,512]{1,0:T(8,128)(2,1)} %val_hbm.1, bf16[512,512]{1,0:T(8,128)(2,1)} %dec_hbm.1, bf16[512,512]{1,0:T(8,128)(2,1)} %learn_hbm.1, bf16[512,2048]{1,0:T(8,128)(2,1)} %wout_hbm.1, ...), custom_call_target="tpu_custom_call" | custom-call | tf_op jit(solution)/shard_map/step/pallas_call | solution.py:445
  152.5 1.9 %copy.23 = bf16[128,2048]{1,0:T(8,128)(2,1)} copy(bf16[128,2048]{1,0:T(8,128)(2,1)} %get-tuple-element.4) | data formatting | bytes 1048576
  154.4 1.9 %copy.24 = bf16[128,2048]{1,0:T(8,128)(2,1)} copy(bf16[128,2048]{1,0:T(8,128)(2,1)} %get-tuple-element.5) | data formatting | bytes 1048576
where the time goes:
time: 157 us; the launch traced here: 156 us
  Pallas kernels  148 us (94%)
  local copies, waits for them, and re-layouts  8.14 us (5%)
    pallas_call x1, Pallas kernels, on_device(): pl.pallas_call(kernel, in_specs=[anywhere] * 10 + [vmem] * 6, out_specs=[...  148 us
    unnamed x5, local copies, waits for them, and re-layouts  8.14 us

commit v1 on v0

--- a/solution.py
+++ b/solution.py
@@ -25,15 +25,14 @@
     r=lax.broadcasted_iota(jnp.int32,(128,128),0); c=lax.broadcasted_iota(jnp.int32,(128,128),1)
     same=(r//64)==(c//64)
     return r,c,same
-def pre_stage(key,dec,learn,base,s0,s1):
+def pre_stage(key,dec,learn,base,shift):
     r,c,same=consts()
     ones=same.astype(B)
     kf=key.astype(F)
     hi,lo=split(kf*kf)
     ss=dg(hi,ones,NN)+dg(lo,ones,NN)
     unit=kf*lax.rsqrt(ss+1e-6)
-    lane=lax.broadcasted_iota(jnp.int32,key.shape,1)
-    pre=dec.astype(F)+base+jnp.where(lane<64,s0,s1)
+    pre=dec.astype(F)+base+shift
     ld=-0.6065306597126334/(1.0+jnp.exp(-pre))
     rem=unit/(1.0+jnp.exp(-learn.astype(F)))
     return kf,unit,ld,rem
@@ -99,9 +98,9 @@
     off=dg(jnp.concatenate([vb,-L],0),jnp.concatenate([BK,BR],0),TN)
     off=jnp.where(same,off*et,zf)
     yield reader,local,T,off
-def local_scan(rec,key,val,dec,learn,base,s0,s1):
+def local_scan(rec,key,val,dec,learn,base,shift):
     n=key.shape[0]//C
-    kf,unit,ld,rem=pre_stage(key,dec,learn,base,s0,s1)
+    kf,unit,ld,rem=pre_stage(key,dec,learn,base,shift)
     cum=chunk_cum(ld)
     outs=[]
     for i in range(n):
@@ -161,24 +160,24 @@
     base_ref, shift_ref, gain_ref, xgain_ref, routes_ref, rw_ref,
     mixer_ref, expert_ref,
     mix_in, wout, xin, g_buf, u_buf, d_buf, rd_buf, lc_buf, mb_buf, row_buf, exc_buf, tz_buf, z_buf, fin_buf, st_buf,
-    wt_buf, out_buf, arr_buf, acc, res_buf, ret_buf, part_buf, rs_buf,
-    in_sems, own_sems, ws, wr, s1, r1, s2, r2, s3, r3, s4, r4, misc, go,
+    wt_buf, out_buf, arr_buf, acc, hid_buf, res_buf, ret_buf, part_buf, rs_buf,
+    in_sems, ws, wr, s1, r1, s2, r2, s3, r3, s4, misc,
 ):
     ep, tp = lax.axis_index("ep"), lax.axis_index("tp")
     z, m = ep // 8, ep % 8
     x, core = m // 2, m % 2
     n = 64
-    right, left = (tp + 1) % 4, (tp + 3) % 4
+    mate, across = tp + 1 - 2 * (tp % 2), 3 - tp
+    other = 1 - 2 * core
+    prime = core == tp // 2
+    client = jnp.where(prime, tp, across)
+    serves = jnp.where(prime, ep, ep + other)
 
     loads = [pltpu.make_async_copy(x_hbm, xin, in_sems.at[0])]
     for i, src in enumerate((rec_hbm, key_hbm, val_hbm, dec_hbm, learn_hbm)):
         loads.append(pltpu.make_async_copy(src, mix_in.at[i], in_sems.at[i + 1]))
     loads.append(pltpu.make_async_copy(wout_hbm, wout, in_sems.at[6]))
-    own = [
-        pltpu.make_async_copy(src, dst.at[0], own_sems.at[i])
-        for i, (src, dst) in enumerate(((gate_hbm, g_buf), (up_hbm, u_buf), (down_hbm, d_buf)))
-    ]
-    for load in loads + own:
+    for load in loads:
         load.start()
 
     barrier = pltpu.get_barrier_semaphore()
@@ -187,79 +186,99 @@
     def _(d):
         pl.semaphore_signal(barrier, inc=1, device_id={"ep": (ep + d) % n}, device_id_type=MESH)
 
-    for d in range(1, 4):
-        pl.semaphore_signal(barrier, inc=1, device_id={"tp": (tp + d) % 4}, device_id_type=MESH)
-    pl.semaphore_wait(barrier, n - 1 + 3)
-
-    half = d_buf.shape[1] // 2
-    top, bottom = pl.ds(0, half), pl.ds(half, half)
-    ahead, back = {"tp": right}, {"tp": left}
-    near = [
-        remote(gate_hbm, g_buf.at[1], ws.at[0], wr.at[0], ahead),
-        remote(up_hbm, u_buf.at[2], ws.at[1], wr.at[1], back),
-        remote(down_hbm, d_buf.at[1], ws.at[2], wr.at[2], ahead),
-        remote(down_hbm, d_buf.at[2], ws.at[3], wr.at[3], back),
-        remote(up_hbm, u_buf.at[1], ws.at[4], wr.at[4], ahead),
-        remote(gate_hbm, g_buf.at[2], ws.at[5], wr.at[5], back),
-    ]
-    far = [
-        remote(g_buf.at[1], g_buf.at[3], ws.at[6], wr.at[6], ahead),
-        remote(u_buf.at[2], u_buf.at[3], ws.at[7], wr.at[7], back),
-        remote(d_buf.at[1, top], d_buf.at[3, top], ws.at[8], wr.at[8], ahead),
-        remote(d_buf.at[2, bottom], d_buf.at[3, bottom], ws.at[9], wr.at[9], back),
-    ]
-
-    def forward():
-        for i in range(4):
-            near[i].wait_recv()
-            far[i].start()
-
-    @pl.when(core == 0)
-    def _():
-        for copy in near:
-            copy.start()
+    @pl.loop(0, n)
+    def _(d):
+        there = {"ep": (ep + d) % n, "tp": across}
+        pl.semaphore_signal(barrier, inc=1, device_id=there, device_id_type=MESH)
+
+    for there in (mate, 3 - mate):
+        pl.semaphore_signal(barrier, inc=1, device_id={"tp": there}, device_id_type=MESH)
+    pl.semaphore_wait(barrier, 2 * n + 1)
+
+    pieces = ((gate_hbm, g_buf), (up_hbm, u_buf), (down_hbm, d_buf))
+    sibling = {"ep": ep + other}
+
+    def put(src, i, slot, sem, where):
+        remote(src, pieces[i][1].at[slot], ws.at[sem], wr.at[3 * slot + i], where).start()
+
+    def land(i, slot):
+        wait_bytes(pieces[i][1].at[slot], wr.at[3 * slot + i])
+
+    def hop(i):
+        @pl.when(prime)
+        def _():
+            land(i, 2)
+            put(pieces[i][1].at[2], i, 3, 6 + i, {"tp": mate})
+            put(pieces[i][1].at[2], i, 2, 9 + i, sibling)
+
+    def share(i, slot):
+        @pl.when(prime)
+        def _():
+            land(i, slot)
+            put(pieces[i][1].at[slot], i, slot, 12 + 3 * (slot // 3) + i, sibling)
+
+    def others_land(i, slot):
+        @pl.when(jnp.logical_not(prime))
+        def _():
+            land(i, slot)
+
+    @pl.when(prime)
+    def _():
+        for i, (src, dst) in enumerate(pieces):
+            put(src, i, 1, i, {"tp": mate})
+        for i, (src, dst) in enumerate(pieces):
+            put(src, i, 0, 3 + i, sibling)
+            pltpu.make_async_copy(src, dst.at[0], wr.at[i]).start()
+
+    @pl.when(jnp.logical_not(prime))
+    def _():
+        for i, (src, dst) in enumerate(pieces):
+            put(src, i, 2, i, {"tp": across})
 
     loads[0].wait()
     rows = xin[...].astype(F)
     normed = (rows * lax.rsqrt(jnp.mean(rows * rows, axis=1, keepdims=True) + NORM_EPS) * xgain_ref[...]).astype(B)
-    named = routes_ref[...]
-    r0, r1_ = named[:, 0:1], named[:, 1:2]
+    r0, r1_ = routes_ref[0:1, :], routes_ref[1:2, :]
     r, c, same = consts()
-    hits = ((c == r0) | (c == r1_)).astype(F).astype(B)
-    earlier = dg((r > c).astype(F).astype(B), hits, NN)
-    t0 = r0.astype(F) * 8.0 + jnp.sum(jnp.where(c == r0, earlier, 0.0), 1, keepdims=True)
-    t1 = r1_.astype(F) * 8.0 + jnp.sum(jnp.where(c == r1_, earlier, 0.0), 1, keepdims=True)
-    place = lax.broadcasted_iota(jnp.int32, (128, n * 8), 1).astype(F)
+    hits = ((r == r0) | (r == r1_)).astype(F).astype(B)
+    earlier = dg(hits, (r < c).astype(F).astype(B), NN)
+    t0 = r0.astype(F) * 8.0 + jnp.sum(jnp.where(r == r0, earlier, 0.0), 0, keepdims=True)
+    t1 = r1_.astype(F) * 8.0 + jnp.sum(jnp.where(r == r1_, earlier, 0.0), 0, keepdims=True)
+    place = lax.broadcasted_iota(jnp.int32, (n * 8, 128), 0).astype(F)
     first, second = place == t0, place == t1
     marks = jnp.where(first | second, 1.0, 0.0).astype(B)
-    shares = jnp.where(first, rw_ref[:, 0:1], 0.0) + jnp.where(second, rw_ref[:, 1:2], 0.0)
-    hi, lo = split(shares)
+    hi, lo = split(jnp.where(first, rw_ref[0:1, :], 0.0) + jnp.where(second, rw_ref[1:2, :], 0.0))
     wt_buf[0] = hi
     wt_buf[1] = lo
     for b in range(4):
         out_buf[16 * b : 16 * b + 16] = (
-            dg(marks[:, 128 * b : 128 * b + 128], normed, TN).reshape(16, 8, -1).astype(B)
+            dg(marks[128 * b : 128 * b + 128], normed, NN).reshape(16, 8, -1).astype(B)
         )
 
-    def send_rows(src, dst, sem, there):
-        remote(src.at[there], dst.at[ep], sem.at[0], sem.at[1], {"ep": there}).start()
+    def dispatch(e):
+        differ = (e % 2 + tp // 2) % 2
+        there = {"ep": e + differ * (1 - 2 * (e % 2)), "tp": tp + differ * (3 - 2 * tp)}
+        remote(out_buf.at[e], arr_buf.at[ep], s4.at[0], s4.at[1], there).start()
 
     @pl.loop(0, n // 2)
     def _(d):
-        send_rows(out_buf, arr_buf, s4, (ep + 2 * d + 1) % n)
+        dispatch((ep + 2 * d + 1) % n)
 
     for load in loads[1:6]:
         load.wait()
+
+    high, rest = split(shift_ref[...])
+    middle, low = split(shift_ref[...] - high.astype(F))
+    shifts = jnp.concatenate([high.astype(F), middle.astype(F), low.astype(F)], 0).astype(B)
 
     @pl.loop(0, 4)
     def _(p):
         lanes = pl.ds(pl.multiple_of(p * 128, 128), 128)
-        shift = shift_ref[...]
-        heads = lax.broadcasted_iota(jnp.int32, shift.shape, 1)
-        h0 = jnp.sum(jnp.where(heads == 2 * p, shift, 0.0), 1, keepdims=True)
-        h1 = jnp.sum(jnp.where(heads == 2 * p + 1, shift, 0.0), 1, keepdims=True)
+        head = lax.broadcasted_iota(jnp.int32, (24, 128), 0) % 8
+        lane = lax.broadcasted_iota(jnp.int32, (24, 128), 1)
+        shift = dg(shifts, (head == 2 * p + lane // 64).astype(F).astype(B), TN)
         a = [mix_in[i, :, lanes] for i in range(5)]
-        rd, lc, whole, offset = local_scan(*a, base_ref[:, lanes], h0, h1)
+        rd, lc, whole, offset = local_scan(*a, base_ref[:, lanes], shift)
         rd_buf[:, lanes] = rd.astype(B)
         lc_buf[:, lanes] = lc
         r, c, same = consts()
@@ -273,10 +292,7 @@
     for d in range(1, 8):
         row_copy(d, m).start()
 
-    @pl.when(core == 0)
-    def _():
-        forward()
-
+    hop(0)
     row_buf[m] = mb_buf[x]
     for d in range(1, 8):
         row_copy(d, (m + d) % 8).wait_recv()
@@ -298,11 +314,19 @@
     for d in range(1, 8):
         z_copy(d, z).start()
 
+    @pl.when(prime)
+    def _():
+        pltpu.make_async_copy(out_buf.at[ep], arr_buf.at[ep], s4.at[1]).start()
+
+    @pl.when(jnp.logical_not(prime))
+    def _():
+        dispatch(ep)
+
     @pl.loop(1, n // 2)
     def _(d):
-        send_rows(out_buf, arr_buf, s4, (ep + 2 * d) % n)
-
-    arr_buf[ep] = out_buf[ep]
+        dispatch((ep + 2 * d) % n)
+
+    hop(1)
     z_buf[z] = tz_buf[...]
     for d in range(1, 8):
         z_copy(d, (z + d) % 8).wait_recv()
@@ -322,11 +346,7 @@
     for d in range(1, 4):
         fin_copy(d, x).start()
 
-    @pl.when(core == 1)
-    def _():
-        for copy in near:
-            copy.start()
-
+    hop(2)
     st_buf[x] = fin_buf[x]
     for d in range(1, 4):
         fin_copy(d, (x + d) % 4).wait_recv()
@@ -344,91 +364,104 @@
             parts.append((centred * lax.rsqrt(variance + GROUP_EPS) * gain_ref[:, lanes]).astype(B))
         part_buf[b] = dg(jnp.concatenate(parts, 1), wout[...], NN).astype(B)
 
-    wait_bytes(arr_buf.at[pl.ds(0, n - 1)], s4.at[1])
-    for copy in own:
-        copy.wait()
-
-    def units(s, b):
+    for i in range(3):
+        share(i, 1)
+    wait_bytes(arr_buf, s4.at[1])
+
+    def hidden(s, b):
         given = arr_buf[pl.ds(16 * b, 16)].reshape(128, -1)
         gate = dg(given, g_buf[s], NN)
         up = dg(given, u_buf[s], NN)
-        hidden = (gate / (1.0 + jnp.exp(-gate)) * up).astype(B)
-        return dg(hidden, d_buf[s], NN)
+        return (gate / (1.0 + jnp.exp(-gate)) * up).astype(B)
+
+    def units(s, b):
+        return dg(hidden(s, b), d_buf[s], NN)
 
     def rows_of(b):
         return pl.ds(pl.multiple_of(b * 128, 128), 128)
+
+    for i in range(3):
+        land(i, 0)
 
     @pl.loop(0, 4)
     def _(b):
         acc[rows_of(b), :] = units(0, b)
 
-    @pl.when(core == 1)
-    def _():
-        forward()
-
-    near[4].wait_recv()
+    for slot in (1, 2):
+        for i in range(3):
+            others_land(i, slot)
+
+        @pl.loop(0, 4)
+        def _(b):
+            acc[rows_of(b), :] += units(slot, b)
+
+    for i in range(2):
+        share(i, 3)
+        others_land(i, 3)
 
     @pl.loop(0, 4)
     def _(b):
-        acc[rows_of(b), :] += units(1, b)
-
-    near[5].wait_recv()
-
-    @pl.loop(0, 4)
-    def _(b):
-        acc[rows_of(b), :] += units(2, b)
-
-    for copy in far:
-        copy.wait_recv()
-
-    @pl.when(core == 1)
-    def _():
-        pl.semaphore_signal(go, inc=1, device_id={"ep": ep - 1}, device_id_type=MESH)
+        hid_buf[rows_of(b), :] = hidden(3, b)
+
+    share(2, 3)
+    others_land(2, 3)
 
     @pl.loop(0, 4)
     def _(i):
         b = (z // 2 + i) % 4
-        res_buf[pl.ds(16 * b, 16)] = (acc[rows_of(b), :] + units(3, b)).reshape(16, 8, -1).astype(B)
+        res_buf[pl.ds(16 * b, 16)] = (
+            (acc[rows_of(b), :] + dg(hid_buf[rows_of(b), :], d_buf[3], NN)).reshape(16, 8, -1).astype(B)
+        )
 
         @pl.loop(0, 16)
         def _(k):
             there = 16 * b + (ep + k) % 16
 
-            @pl.when(there != ep)
+            @pl.when(jnp.logical_or(there != ep, jnp.logical_not(prime)))
             def _():
-                send_rows(res_buf, ret_buf, misc, there)
-
-    @pl.when(core == 0)
-    def _():
-        pl.semaphore_wait(go, 1)
+                where = {"ep": there, "tp": client}
+                remote(res_buf.at[there], ret_buf.at[serves], misc.at[0], misc.at[1], where).start()
+
+    @pl.when(prime)
+    def _():
+        pltpu.make_async_copy(res_buf.at[ep], ret_buf.at[ep], misc.at[1]).start()
 
     def rs_copy(d, slot):
         j = (tp + d) % 4
-        return remote(part_buf.at[j], rs_buf.at[slot], ws.at[9 + d], wr.at[10 + slot], {"tp": j})
+        return remote(part_buf.at[j], rs_buf.at[slot], ws.at[17 + d], wr.at[12 + slot], {"tp": j})
 
     for d in range(1, 4):
         rs_copy(d, tp).start()
-    ret_buf[ep] = res_buf[ep]
     total = part_buf[tp].astype(F)
     for d in range(1, 4):
         rs_copy(d, (tp + d) % 4).wait_recv()
         total += rs_buf[(tp + d) % 4].astype(F)
     mixer_ref[...] = total.astype(B)
 
-    wait_bytes(ret_buf.at[pl.ds(0, n - 1)], misc.at[1])
+    wait_bytes(ret_buf, misc.at[1])
     back_rows = ret_buf[...].reshape(n * 8, -1)
-    expert_ref[...] = (dg(wt_buf[0], back_rows, NN) + dg(wt_buf[1], back_rows, NN)).astype(B)
-
-    for copy in near + far:
-        copy.wait_send()
+    expert_ref[...] = (dg(wt_buf[0], back_rows, TN) + dg(wt_buf[1], back_rows, TN)).astype(B)
+
     for d in range(1, 8):
         row_copy(d, m).wait_send()
         z_copy(d, z).wait_send()
     for d in range(1, 4):
         fin_copy(d, x).wait_send()
         rs_copy(d, tp).wait_send()
-    wait_bytes(out_buf.at[pl.ds(0, n - 1)], s4.at[0])
-    wait_bytes(res_buf.at[pl.ds(0, n - 1)], misc.at[0])
+
+    def sent(count, rows_sent):
+        for k in range(count):
+            wait_bytes(pieces[k % 3][1].at[0], ws.at[k])
+        wait_bytes(out_buf.at[pl.ds(0, rows_sent)], s4.at[0])
+        wait_bytes(res_buf.at[pl.ds(0, rows_sent)], misc.at[0])
+
+    @pl.when(prime)
+    def _():
+        sent(18, n - 1)
+
+    @pl.when(jnp.logical_not(prime))
+    def _():
+        sent(3, n)
 
 
 def on_device(
@@ -453,10 +486,10 @@
             V((rows, channels), B), V((rows, channels), F),
             V((4, 128, 128), B), V((8, 128, 128), B), V((8, 128, 128), F), V((128, 128), B), V((8, 128, 128), B),
             V((4, C, 128), B), V((4, C, 128), B),
-            V((2, t, 512), B), V((64, 8, width), B), V((64, 8, width), B), V((512, width), F),
+            V((2, 512, t), B), V((64, 8, width), B), V((64, 8, width), B), V((512, width), F), V((512, units), B),
             V((64, 8, width), B), V((64, 8, width), B), V((4, t, width), B), V((4, t, width), B),
-            dma((7,)), dma((3,)), dma((13,)), dma((14,)), dma((8,)), dma((8,)), dma((8,)), dma((8,)), dma((4,)), dma((4,)),
-            dma((2,)), dma((2,)), dma((2,)), pltpu.SemaphoreType.REGULAR,
+            dma((7,)), dma((21,)), dma((16,)), dma((8,)), dma((8,)), dma((8,)), dma((8,)), dma((4,)), dma((4,)),
+            dma((2,)), dma((2,)),
         ],
         compiler_params=pltpu.CompilerParams(
             collective_id=0, has_side_effects=True, vmem_limit_bytes=60 * 1024 * 1024
@@ -465,8 +498,8 @@
     )(
         receptance, key_rows, value_rows, decay_input, learn_input, out_weight, expert_input,
         gate_weight[0], up_weight[0], down_weight[0],
-        decay_base.reshape(1, channels), decay_shift, channel_gain.reshape(1, channels), expert_gain.reshape(1, width),
-        routes, route_weight,
+        decay_base.reshape(1, channels), decay_shift.T, channel_gain.reshape(1, channels), expert_gain.reshape(1, width),
+        routes.T, route_weight.T,
     )
 
 

time: 157 us -> 145 us (0.924)
  Pallas kernels: 148 us -> 140 us
  local copies, waits for them, and re-layouts: 8.14 us -> 3.76 us
    pallas_call x1, Pallas kernels: 148 us -> 140 us  [on_device(): pl.pallas_call(kernel, in_specs=[anywhere] * 10 + [vmem] * 6, out_specs=[...]
    unnamed x5 -> x2, local copies, waits for them, and re-layouts: 8.14 us -> 3.76 us
where the time goes in v1:
time: 145 us
  Pallas kernels  140 us (97%)
  local copies, waits for them, and re-layouts  3.76 us (3%)
    pallas_call x1, Pallas kernels, on_device(): pl.pallas_call(kernel, in_specs=[anywhere] * 10 + [vmem] * 6, out_specs=[...  140 us
    unnamed x2, local copies, waits for them, and re-layouts  3.76 us

profile of v1, /device:TPU:1, one launch (start us, length us, event | category | flops | bytes accessed | tf_op | source)
XLA Modules:
  0.0 144.7 jit_solution(18233191811341740031)
XLA Ops:
  0.6 140.3 %step.1 = (bf16[128,2048]{1,0:T(8,128)(2,1)}, bf16[128,2048]{1,0:T(8,128)(2,1)}) custom-call(bf16[512,512]{1,0:T(8,128)(2,1)} %rec_hbm.1, bf16[512,512]{1,0:T(8,128)(2,1)} %key_hbm.1, bf16[512,512]{1,0:T(8,128)(2,1)} %val_hbm.1, bf16[512,512]{1,0:T(8,128)(2,1)} %dec_hbm.1, bf16[512,512]{1,0:T(8,128)(2,1)} %learn_hbm.1, bf16[512,2048]{1,0:T(8,128)(2,1)} %wout_hbm.1, ...), custom_call_target="tpu_custom_call" | custom-call | tf_op jit(solution)/shard_map/step/pallas_call | solution.py:478
  140.9 1.9 %copy.20 = bf16[128,2048]{1,0:T(8,128)(2,1)} copy(bf16[128,2048]{1,0:T(8,128)(2,1)} %get-tuple-element.4) | data formatting | bytes 1048576
  142.8 1.9 %copy.21 = bf16[128,2048]{1,0:T(8,128)(2,1)} copy(bf16[128,2048]{1,0:T(8,128)(2,1)} %get-tuple-element.5) | data formatting | bytes 1048576

commit v2 on v1

--- a/solution.py
+++ b/solution.py
@@ -145,6 +145,17 @@
     return dg(hi, ones, NN) + dg(lo, ones, NN)
 
 
+def places(routes_ref, experts):
+    r0, r1 = routes_ref[0:1, :], routes_ref[1:2, :]
+    r, c, same = consts()
+    hits = ((r == r0) | (r == r1)).astype(F).astype(B)
+    earlier = dg(hits, (r < c).astype(F).astype(B), NN)
+    t0 = r0.astype(F) * 8.0 + jnp.sum(jnp.where(r == r0, earlier, 0.0), 0, keepdims=True)
+    t1 = r1.astype(F) * 8.0 + jnp.sum(jnp.where(r == r1, earlier, 0.0), 0, keepdims=True)
+    place = lax.broadcasted_iota(jnp.int32, (experts * 8, 128), 0).astype(F)
+    return place == t0, place == t1
+
+
 def remote(src, dst, send, recv, where):
     return pltpu.make_async_remote_copy(
         src_ref=src, dst_ref=dst, send_sem=send, recv_sem=recv, device_id=where, device_id_type=MESH
@@ -157,10 +168,10 @@
 
 def kernel(
     rec_hbm, key_hbm, val_hbm, dec_hbm, learn_hbm, wout_hbm, x_hbm, gate_hbm, up_hbm, down_hbm,
-    base_ref, shift_ref, gain_ref, xgain_ref, routes_ref, rw_ref,
-    mixer_ref, expert_ref,
+    base_ref, shift_ref, gain_ref, xgain_ref, routes_ref,
+    mixer_ref, ret_buf,
     mix_in, wout, xin, g_buf, u_buf, d_buf, rd_buf, lc_buf, mb_buf, row_buf, exc_buf, tz_buf, z_buf, fin_buf, st_buf,
-    wt_buf, out_buf, arr_buf, acc, hid_buf, res_buf, ret_buf, part_buf, rs_buf,
+    out_buf, arr_buf, acc, hid_buf, res_buf, part_buf, rs_buf,
     in_sems, ws, wr, s1, r1, s2, r2, s3, r3, s4, misc,
 ):
     ep, tp = lax.axis_index("ep"), lax.axis_index("tp")
@@ -182,17 +193,28 @@
 
     barrier = pltpu.get_barrier_semaphore()
 
-    @pl.loop(1, n)
+    @pl.loop(1, n, unroll=9)
     def _(d):
         pl.semaphore_signal(barrier, inc=1, device_id={"ep": (ep + d) % n}, device_id_type=MESH)
 
-    @pl.loop(0, n)
+    @pl.loop(0, n, unroll=8)
     def _(d):
         there = {"ep": (ep + d) % n, "tp": across}
         pl.semaphore_signal(barrier, inc=1, device_id=there, device_id_type=MESH)
 
     for there in (mate, 3 - mate):
         pl.semaphore_signal(barrier, inc=1, device_id={"tp": there}, device_id_type=MESH)
+    loads[0].wait()
+    rows = xin[...].astype(F)
+    normed = (rows * lax.rsqrt(jnp.mean(rows * rows, axis=1, keepdims=True) + NORM_EPS) * xgain_ref[...]).astype(B)
+    first, second = places(routes_ref, n)
+    marks = jnp.where(first | second, 1.0, 0.0).astype(B)
+    r, c, same = consts()
+    for b in range(4):
+        out_buf[16 * b : 16 * b + 16] = (
+            dg(marks[128 * b : 128 * b + 128], normed, NN).reshape(16, 8, -1).astype(B)
+        )
+
     pl.semaphore_wait(barrier, 2 * n + 1)
 
     pieces = ((gate_hbm, g_buf), (up_hbm, u_buf), (down_hbm, d_buf))
@@ -203,12 +225,25 @@
 
     def land(i, slot):
         wait_bytes(pieces[i][1].at[slot], wr.at[3 * slot + i])
+
+    half = d_buf.shape[1] // 2
+    halves = (pl.ds(0, half), pl.ds(half, half))
+
+    def last(src, h, sem, where):
+        remote(src, d_buf.at[3, halves[h]], ws.at[sem], wr.at[(11, 16)[h]], where).start()
+
+    def last_land(h):
+        wait_bytes(d_buf.at[3, halves[h]], wr.at[(11, 16)[h]])
 
     def hop(i):
         @pl.when(prime)
         def _():
             land(i, 2)
-            put(pieces[i][1].at[2], i, 3, 6 + i, {"tp": mate})
+            if i < 2:
+                put(pieces[i][1].at[2], i, 3, 6 + i, {"tp": mate})
+            else:
+                for h in range(2):
+                    last(d_buf.at[2, halves[h]], h, (8, 21)[h], {"tp": mate})
             put(pieces[i][1].at[2], i, 2, 9 + i, sibling)
 
     def share(i, slot):
@@ -234,26 +269,6 @@
     def _():
         for i, (src, dst) in enumerate(pieces):
             put(src, i, 2, i, {"tp": across})
-
-    loads[0].wait()
-    rows = xin[...].astype(F)
-    normed = (rows * lax.rsqrt(jnp.mean(rows * rows, axis=1, keepdims=True) + NORM_EPS) * xgain_ref[...]).astype(B)
-    r0, r1_ = routes_ref[0:1, :], routes_ref[1:2, :]
-    r, c, same = consts()
-    hits = ((r == r0) | (r == r1_)).astype(F).astype(B)
-    earlier = dg(hits, (r < c).astype(F).astype(B), NN)
-    t0 = r0.astype(F) * 8.0 + jnp.sum(jnp.where(r == r0, earlier, 0.0), 0, keepdims=True)
-    t1 = r1_.astype(F) * 8.0 + jnp.sum(jnp.where(r == r1_, earlier, 0.0), 0, keepdims=True)
-    place = lax.broadcasted_iota(jnp.int32, (n * 8, 128), 0).astype(F)
-    first, second = place == t0, place == t1
-    marks = jnp.where(first | second, 1.0, 0.0).astype(B)
-    hi, lo = split(jnp.where(first, rw_ref[0:1, :], 0.0) + jnp.where(second, rw_ref[1:2, :], 0.0))
-    wt_buf[0] = hi
-    wt_buf[1] = lo
-    for b in range(4):
-        out_buf[16 * b : 16 * b + 16] = (
-            dg(marks[128 * b : 128 * b + 128], normed, NN).reshape(16, 8, -1).astype(B)
-        )
 
     def dispatch(e):
         differ = (e % 2 + tp // 2) % 2
@@ -291,6 +306,10 @@
 
     for d in range(1, 8):
         row_copy(d, m).start()
+
+    @pl.loop(1, n // 4)
+    def _(d):
+        dispatch((ep + 4 * d) % n)
 
     hop(0)
     row_buf[m] = mb_buf[x]
@@ -322,11 +341,13 @@
     def _():
         dispatch(ep)
 
-    @pl.loop(1, n // 2)
+    @pl.loop(0, n // 4)
     def _(d):
-        dispatch((ep + 2 * d) % n)
+        dispatch((ep + 4 * d + 2) % n)
 
     hop(1)
+    for i in range(3):
+        share(i, 1)
     z_buf[z] = tz_buf[...]
     for d in range(1, 8):
         z_copy(d, (z + d) % 8).wait_recv()
@@ -346,7 +367,6 @@
     for d in range(1, 4):
         fin_copy(d, x).start()
 
-    hop(2)
     st_buf[x] = fin_buf[x]
     for d in range(1, 4):
         fin_copy(d, (x + d) % 4).wait_recv()
@@ -364,8 +384,16 @@
             parts.append((centred * lax.rsqrt(variance + GROUP_EPS) * gain_ref[:, lanes]).astype(B))
         part_buf[b] = dg(jnp.concatenate(parts, 1), wout[...], NN).astype(B)
 
-    for i in range(3):
-        share(i, 1)
+    hop(2)
+    def rs_copy(d, slot):
+        j = (tp + d) % 4
+        return remote(part_buf.at[j], rs_buf.at[slot], ws.at[17 + d], wr.at[12 + slot], {"tp": j})
+
+    def rs_to(j):
+        return remote(part_buf.at[j], rs_buf.at[tp], ws.at[18 + (j - tp + 3) % 4], wr.at[12 + tp], {"tp": j})
+
+    rs_to(across).start()
+
     wait_bytes(arr_buf, s4.at[1])
 
     def hidden(s, b):
@@ -387,7 +415,7 @@
     def _(b):
         acc[rows_of(b), :] = units(0, b)
 
-    for slot in (1, 2):
+    def add_slot(slot):
         for i in range(3):
             others_land(i, slot)
 
@@ -395,6 +423,8 @@
         def _(b):
             acc[rows_of(b), :] += units(slot, b)
 
+    add_slot(1)
+    add_slot(2)
     for i in range(2):
         share(i, 3)
         others_land(i, 3)
@@ -403,12 +433,19 @@
     def _(b):
         hid_buf[rows_of(b), :] = hidden(3, b)
 
-    share(2, 3)
-    others_land(2, 3)
+    for h in range(2):
+        last_land(h)
+
+        @pl.when(prime)
+        def _():
+            last(d_buf.at[3, halves[h]], h, (17, 22)[h], sibling)
+
+    rs_to(mate).start()
+    rs_to(3 - mate).start()
 
     @pl.loop(0, 4)
     def _(i):
-        b = (z // 2 + i) % 4
+        b = (z // 2 + 2 + i) % 4
         res_buf[pl.ds(16 * b, 16)] = (
             (acc[rows_of(b), :] + dg(hid_buf[rows_of(b), :], d_buf[3], NN)).reshape(16, 8, -1).astype(B)
         )
@@ -426,22 +463,15 @@
     def _():
         pltpu.make_async_copy(res_buf.at[ep], ret_buf.at[ep], misc.at[1]).start()
 
-    def rs_copy(d, slot):
-        j = (tp + d) % 4
-        return remote(part_buf.at[j], rs_buf.at[slot], ws.at[17 + d], wr.at[12 + slot], {"tp": j})
-
-    for d in range(1, 4):
-        rs_copy(d, tp).start()
     total = part_buf[tp].astype(F)
     for d in range(1, 4):
         rs_copy(d, (tp + d) % 4).wait_recv()
         total += rs_buf[(tp + d) % 4].astype(F)
-    mixer_ref[...] = total.astype(B)
+    xin[...] = total.astype(B)
+    leave = [pltpu.make_async_copy(xin, mixer_ref, in_sems.at[0])]
+    leave[0].start()
 
     wait_bytes(ret_buf, misc.at[1])
-    back_rows = ret_buf[...].reshape(n * 8, -1)
-    expert_ref[...] = (dg(wt_buf[0], back_rows, TN) + dg(wt_buf[1], back_rows, TN)).astype(B)
-
     for d in range(1, 8):
         row_copy(d, m).wait_send()
         z_copy(d, z).wait_send()
@@ -451,7 +481,11 @@
 
     def sent(count, rows_sent):
         for k in range(count):
-            wait_bytes(pieces[k % 3][1].at[0], ws.at[k])
+            if k not in (8, 17):
+                wait_bytes(pieces[k % 3][1].at[0], ws.at[k])
+            else:
+                for sem in (k, 21 + k // 17):
+                    wait_bytes(d_buf.at[0, halves[0]], ws.at[sem])
         wait_bytes(out_buf.at[pl.ds(0, rows_sent)], s4.at[0])
         wait_bytes(res_buf.at[pl.ds(0, rows_sent)], misc.at[0])
 
@@ -462,6 +496,31 @@
     @pl.when(jnp.logical_not(prime))
     def _():
         sent(3, n)
+    for copy in leave:
+        copy.wait()
+
+
+def finish_kernel(mixed, returned, routes_ref, rw_ref, mixer_ref, expert_ref, rows, mix, out, loaded, stored):
+    count, width = rows.shape[0], rows.shape[2]
+    parts = [pl.ds(width // 4 * k, width // 4) for k in range(4)]
+    loads = [pltpu.make_async_copy(returned.at[:, :, p], rows.at[:, :, p], loaded.at[k]) for k, p in enumerate(parts)]
+    loads.append(pltpu.make_async_copy(mixed, mix, loaded.at[4]))
+    for load in loads:
+        load.start()
+    first, second = places(routes_ref, count)
+    hi, lo = split(jnp.where(first, rw_ref[0:1, :], 0.0) + jnp.where(second, rw_ref[1:2, :], 0.0))
+    stores = []
+    for k, p in enumerate(parts):
+        loads[k].wait()
+        given = rows[:, :, p].reshape(count * 8, -1)
+        out[:, p] = (dg(hi, given, TN) + dg(lo, given, TN)).astype(B)
+        stores.append(pltpu.make_async_copy(out.at[:, p], expert_ref.at[:, p], stored.at[k]))
+        stores[k].start()
+    loads[4].wait()
+    stores.append(pltpu.make_async_copy(mix, mixer_ref, stored.at[4]))
+    stores[4].start()
+    for store in stores:
+        store.wait()
 
 
 def on_device(
@@ -472,23 +531,24 @@
     rows, channels = receptance.shape
     depth, units = gate_weight.shape[1:]
     vmem = pl.BlockSpec(memory_space=pltpu.VMEM)
-    anywhere = pl.BlockSpec(memory_space=pl.ANY)
+    anywhere = pl.BlockSpec(memory_space=pltpu.HBM)
     dma = pltpu.SemaphoreType.DMA
     V = pltpu.VMEM
-    return pl.pallas_call(
+    both = jax.ShapeDtypeStruct((t, width), B)
+    mixed, returned = pl.pallas_call(
         kernel,
-        in_specs=[anywhere] * 10 + [vmem] * 6,
-        out_specs=[vmem, vmem],
-        out_shape=[jax.ShapeDtypeStruct((t, width), B)] * 2,
+        in_specs=[anywhere] * 10 + [vmem] * 5,
+        out_specs=[anywhere, anywhere],
+        out_shape=[both, jax.ShapeDtypeStruct((64, 8, width), B)],
         scratch_shapes=[
             V((5, rows, channels), B), V((channels, width), B), V((t, width), B),
             V((4, depth, units), B), V((4, depth, units), B), V((4, units, width), B),
             V((rows, channels), B), V((rows, channels), F),
             V((4, 128, 128), B), V((8, 128, 128), B), V((8, 128, 128), F), V((128, 128), B), V((8, 128, 128), B),
             V((4, C, 128), B), V((4, C, 128), B),
-            V((2, 512, t), B), V((64, 8, width), B), V((64, 8, width), B), V((512, width), F), V((512, units), B),
-            V((64, 8, width), B), V((64, 8, width), B), V((4, t, width), B), V((4, t, width), B),
-            dma((7,)), dma((21,)), dma((16,)), dma((8,)), dma((8,)), dma((8,)), dma((8,)), dma((4,)), dma((4,)),
+            V((64, 8, width), B), V((64, 8, width), B), V((512, width), F), V((512, units), B),
+            V((64, 8, width), B), V((4, t, width), B), V((4, t, width), B),
+            dma((7,)), dma((23,)), dma((17,)), dma((8,)), dma((8,)), dma((8,)), dma((8,)), dma((4,)), dma((4,)),
             dma((2,)), dma((2,)),
         ],
         compiler_params=pltpu.CompilerParams(
@@ -499,8 +559,16 @@
         receptance, key_rows, value_rows, decay_input, learn_input, out_weight, expert_input,
         gate_weight[0], up_weight[0], down_weight[0],
         decay_base.reshape(1, channels), decay_shift.T, channel_gain.reshape(1, channels), expert_gain.reshape(1, width),
-        routes.T, route_weight.T,
+        routes.T,
     )
+    return pl.pallas_call(
+        finish_kernel,
+        in_specs=[anywhere, anywhere, vmem, vmem],
+        out_specs=[anywhere, anywhere],
+        out_shape=[both, both],
+        scratch_shapes=[V((64, 8, width), B), V((t, width), B), V((t, width), B), dma((5,)), dma((5,))],
+        name="finish",
+    )(mixed, returned, routes.T, route_weight.T)
 
 
 def solution(mesh):

time: 145 us -> 140 us (0.966)
  local copies, waits for them, and re-layouts: 3.76 us -> 0 us
    unnamed x2 -> x0, local copies, waits for them, and re-layouts: 3.76 us -> none
    pallas_call x1 -> x2, Pallas kernels: 140 us -> 139 us  [the longest x1 135 us: on_device(): pl.pallas_call(kernel, in_specs=[anywhere] * 10 + [vmem] * 5, out_specs=[...]
where the time goes in v2:
time: 140 us
  Pallas kernels  139 us (99%)
    pallas_call x1, Pallas kernels, on_device(): pl.pallas_call(kernel, in_specs=[anywhere] * 10 + [vmem] * 5, out_specs=[...  135 us
    pallas_call x1, Pallas kernels, on_device(): pl.pallas_call(finish_kernel, in_specs=[anywhere, anywhere, vmem, vmem],...  3.93 us

profile of v2, /device:TPU:1, one launch (start us, length us, event | category | flops | bytes accessed | tf_op | source)
XLA Modules:
  0.0 139.7 jit_solution(7984568648611107470)
XLA Ops:
  0.6 134.9 %step.1 = (bf16[128,2048]{1,0:T(8,128)(2,1)}, bf16[64,8,2048]{2,1,0:T(8,128)(2,1)}) custom-call(bf16[512,512]{1,0:T(8,128)(2,1)} %rec_hbm.1, bf16[512,512]{1,0:T(8,128)(2,1)} %key_hbm.1, bf16[512,512]{1,0:T(8,128)(2,1)} %val_hbm.1, bf16[512,512]{1,0:T(8,128)(2,1)} %dec_hbm.1, bf16[512,512]{1,0:T(8,128)(2,1)} %learn_hbm.1, bf16[512,2048]{1,0:T(8,128)(2,1)} %wout_hbm.1, ...), custom_call_target="tpu_custom_call" | custom-call | tf_op jit(solution)/shard_map/step/pallas_call | solution.py:538
  135.6 3.9 %finish.1 = (bf16[128,2048]{1,0:T(8,128)(2,1)}, bf16[128,2048]{1,0:T(8,128)(2,1)}) custom-call(bf16[128,2048]{1,0:T(8,128)(2,1)} %get-tuple-element.4.mixed, bf16[64,8,2048]{2,1,0:T(8,128)(2,1)} %get-tuple-element.5.returned, s32[2,128]{1,0:T(2,128)} %bitcast.15, f32[2,128]{1,0:T(2,128)} %bitcast.18), custom_call_target="tpu_custom_call" | custom-call | tf_op jit(solution)/shard_map/finish/pallas_call | solution.py:564

commit v3 on v2

--- a/solution.py
+++ b/solution.py
@@ -166,10 +166,14 @@
     pltpu.make_async_copy(ref, ref, sem).wait()
 
 
+ORDER = ((1, 7), (2, 6), (3, 5), (0, 4))
+
+
 def kernel(
     rec_hbm, key_hbm, val_hbm, dec_hbm, learn_hbm, wout_hbm, x_hbm, gate_hbm, up_hbm, down_hbm,
+    base_hbm, shift_hbm, gain_hbm, xgain_hbm, routes_hbm,
+    mixer_ref, ret_buf,
     base_ref, shift_ref, gain_ref, xgain_ref, routes_ref,
-    mixer_ref, ret_buf,
     mix_in, wout, xin, g_buf, u_buf, d_buf, rd_buf, lc_buf, mb_buf, row_buf, exc_buf, tz_buf, z_buf, fin_buf, st_buf,
     out_buf, arr_buf, acc, hid_buf, res_buf, part_buf, rs_buf,
     in_sems, ws, wr, s1, r1, s2, r2, s3, r3, s4, misc,
@@ -184,11 +188,13 @@
     client = jnp.where(prime, tp, across)
     serves = jnp.where(prime, ep, ep + other)
 
+    smalls = ((routes_hbm, routes_ref), (xgain_hbm, xgain_ref), (base_hbm, base_ref), (shift_hbm, shift_ref), (gain_hbm, gain_ref))
+    small = [pltpu.make_async_copy(src, dst, in_sems.at[7 + i]) for i, (src, dst) in enumerate(smalls)]
     loads = [pltpu.make_async_copy(x_hbm, xin, in_sems.at[0])]
     for i, src in enumerate((rec_hbm, key_hbm, val_hbm, dec_hbm, learn_hbm)):
         loads.append(pltpu.make_async_copy(src, mix_in.at[i], in_sems.at[i + 1]))
     loads.append(pltpu.make_async_copy(wout_hbm, wout, in_sems.at[6]))
-    for load in loads:
+    for load in small[:2] + loads[:1] + small[2:] + loads[1:]:
         load.start()
 
     barrier = pltpu.get_barrier_semaphore()
@@ -204,7 +210,8 @@
 
     for there in (mate, 3 - mate):
         pl.semaphore_signal(barrier, inc=1, device_id={"tp": there}, device_id_type=MESH)
-    loads[0].wait()
+    for load in small[:2] + loads[:1]:
+        load.wait()
     rows = xin[...].astype(F)
     normed = (rows * lax.rsqrt(jnp.mean(rows * rows, axis=1, keepdims=True) + NORM_EPS) * xgain_ref[...]).astype(B)
     first, second = places(routes_ref, n)
@@ -279,7 +286,7 @@
     def _(d):
         dispatch((ep + 2 * d + 1) % n)
 
-    for load in loads[1:6]:
+    for load in small[2:] + loads[1:6]:
         load.wait()
 
     high, rest = split(shift_ref[...])
@@ -393,6 +400,7 @@
         return remote(part_buf.at[j], rs_buf.at[tp], ws.at[18 + (j - tp + 3) % 4], wr.at[12 + tp], {"tp": j})
 
     rs_to(across).start()
+    share(0, 3)
 
     wait_bytes(arr_buf, s4.at[1])
 
@@ -424,9 +432,9 @@
             acc[rows_of(b), :] += units(slot, b)
 
     add_slot(1)
+    share(1, 3)
     add_slot(2)
     for i in range(2):
-        share(i, 3)
         others_land(i, 3)
 
     @pl.loop(0, 4)
@@ -443,16 +451,17 @@
     rs_to(mate).start()
     rs_to(3 - mate).start()
 
-    @pl.loop(0, 4)
-    def _(i):
-        b = (z // 2 + 2 + i) % 4
-        res_buf[pl.ds(16 * b, 16)] = (
-            (acc[rows_of(b), :] + dg(hid_buf[rows_of(b), :], d_buf[3], NN)).reshape(16, 8, -1).astype(B)
-        )
+    for offsets in ORDER:
+        two = [(z + o) % 8 for o in offsets]
+        block = [pl.ds(pl.multiple_of(64 * there, 64), 64) for there in two]
+        low_part = dg(jnp.concatenate([hid_buf[b, :] for b in block], 0), d_buf[3], NN)
+        for k, (there, b) in enumerate(zip(two, block)):
+            full = acc[b, :] + low_part[64 * k : 64 * k + 64]
+            res_buf[pl.ds(8 * there, 8)] = full.reshape(8, 8, -1).astype(B)
 
         @pl.loop(0, 16)
         def _(k):
-            there = 16 * b + (ep + k) % 16
+            there = 8 * ((z + offsets[0] + (k % 2) * (offsets[1] - offsets[0])) % 8) + (m + k // 2) % 8
 
             @pl.when(jnp.logical_or(there != ep, jnp.logical_not(prime)))
             def _():
@@ -500,13 +509,18 @@
         copy.wait()
 
 
-def finish_kernel(mixed, returned, routes_ref, rw_ref, mixer_ref, expert_ref, rows, mix, out, loaded, stored):
+def finish_kernel(mixed, returned, routes_hbm, rw_hbm, mixer_ref, expert_ref, routes_ref, rw_ref, rows, mix, out, loaded, stored):
     count, width = rows.shape[0], rows.shape[2]
     parts = [pl.ds(width // 4 * k, width // 4) for k in range(4)]
     loads = [pltpu.make_async_copy(returned.at[:, :, p], rows.at[:, :, p], loaded.at[k]) for k, p in enumerate(parts)]
     loads.append(pltpu.make_async_copy(mixed, mix, loaded.at[4]))
-    for load in loads:
+    small = [
+        pltpu.make_async_copy(routes_hbm, routes_ref, loaded.at[5]), pltpu.make_async_copy(rw_hbm, rw_ref, loaded.at[6])
+    ]
+    for load in small + loads:
         load.start()
+    for load in small:
+        load.wait()
     first, second = places(routes_ref, count)
     hi, lo = split(jnp.where(first, rw_ref[0:1, :], 0.0) + jnp.where(second, rw_ref[1:2, :], 0.0))
     stores = []
@@ -516,9 +530,11 @@
         out[:, p] = (dg(hi, given, TN) + dg(lo, given, TN)).astype(B)
         stores.append(pltpu.make_async_copy(out.at[:, p], expert_ref.at[:, p], stored.at[k]))
         stores[k].start()
-    loads[4].wait()
-    stores.append(pltpu.make_async_copy(mix, mixer_ref, stored.at[4]))
-    stores[4].start()
+        if k == 1:
+            loads[4].wait()
+            leave = pltpu.make_async_copy(mix, mixer_ref, stored.at[4])
+            leave.start()
+    stores.append(leave)
     for store in stores:
         store.wait()
 
@@ -530,17 +546,17 @@
     t, width = expert_input.shape
     rows, channels = receptance.shape
     depth, units = gate_weight.shape[1:]
-    vmem = pl.BlockSpec(memory_space=pltpu.VMEM)
     anywhere = pl.BlockSpec(memory_space=pltpu.HBM)
     dma = pltpu.SemaphoreType.DMA
     V = pltpu.VMEM
     both = jax.ShapeDtypeStruct((t, width), B)
     mixed, returned = pl.pallas_call(
         kernel,
-        in_specs=[anywhere] * 10 + [vmem] * 5,
+        in_specs=[anywhere] * 15,
         out_specs=[anywhere, anywhere],
         out_shape=[both, jax.ShapeDtypeStruct((64, 8, width), B)],
         scratch_shapes=[
+            V((1, channels), F), V((8, rows), F), V((1, channels), F), V((1, width), F), V((2, t), jnp.int32),
             V((5, rows, channels), B), V((channels, width), B), V((t, width), B),
             V((4, depth, units), B), V((4, depth, units), B), V((4, units, width), B),
             V((rows, channels), B), V((rows, channels), F),
@@ -548,7 +564,7 @@
             V((4, C, 128), B), V((4, C, 128), B),
             V((64, 8, width), B), V((64, 8, width), B), V((512, width), F), V((512, units), B),
             V((64, 8, width), B), V((4, t, width), B), V((4, t, width), B),
-            dma((7,)), dma((23,)), dma((17,)), dma((8,)), dma((8,)), dma((8,)), dma((8,)), dma((4,)), dma((4,)),
+            dma((12,)), dma((23,)), dma((17,)), dma((8,)), dma((8,)), dma((8,)), dma((8,)), dma((4,)), dma((4,)),
             dma((2,)), dma((2,)),
         ],
         compiler_params=pltpu.CompilerParams(
@@ -563,10 +579,12 @@
     )
     return pl.pallas_call(
         finish_kernel,
-        in_specs=[anywhere, anywhere, vmem, vmem],
+        in_specs=[anywhere] * 4,
         out_specs=[anywhere, anywhere],
         out_shape=[both, both],
-        scratch_shapes=[V((64, 8, width), B), V((t, width), B), V((t, width), B), dma((5,)), dma((5,))],
+        scratch_shapes=[
+            V((2, t), jnp.int32), V((2, t), F), V((64, 8, width), B), V((t, width), B), V((t, width), B), dma((7,)), dma((5,)),
+        ],
         name="finish",
     )(mixed, returned, routes.T, route_weight.T)
 

time: 140 us -> 139 us (level)
  Pallas kernels: 139 us -> 137 us
    pallas_call x2, Pallas kernels: 139 us -> 137 us  [the longest x1 134 us: on_device(): pl.pallas_call(kernel, in_specs=[anywhere] * 15, out_specs=[anywhere, any...]
where the time goes in v3:
time: 139 us; the launch traced here: 138 us
  Pallas kernels  137 us (99%)
    pallas_call x1, Pallas kernels, on_device(): pl.pallas_call(kernel, in_specs=[anywhere] * 15, out_specs=[anywhere, any...  134 us
    pallas_call x1, Pallas kernels, on_device(): pl.pallas_call(finish_kernel, in_specs=[anywhere] * 4, out_specs=[anywher...  3.13 us

profile of v3, /device:TPU:1, one launch (start us, length us, event | category | flops | bytes accessed | tf_op | source)
XLA Modules:
  0.0 137.7 jit_solution(2003742316259967986)
XLA Ops:
  0.6 133.7 %step.1 = (bf16[128,2048]{1,0:T(8,128)(2,1)}, bf16[64,8,2048]{2,1,0:T(8,128)(2,1)}) custom-call(bf16[512,512]{1,0:T(8,128)(2,1)} %rec_hbm.1, bf16[512,512]{1,0:T(8,128)(2,1)} %key_hbm.1, bf16[512,512]{1,0:T(8,128)(2,1)} %val_hbm.1, bf16[512,512]{1,0:T(8,128)(2,1)} %dec_hbm.1, bf16[512,512]{1,0:T(8,128)(2,1)} %learn_hbm.1, bf16[512,2048]{1,0:T(8,128)(2,1)} %wout_hbm.1, ...), custom_call_target="tpu_custom_call" | custom-call | tf_op jit(solution)/shard_map/step/pallas_call | solution.py:553
  134.4 3.1 %finish.1 = (bf16[128,2048]{1,0:T(8,128)(2,1)}, bf16[128,2048]{1,0:T(8,128)(2,1)}) custom-call(bf16[128,2048]{1,0:T(8,128)(2,1)} %get-tuple-element.4.mixed, bf16[64,8,2048]{2,1,0:T(8,128)(2,1)} %get-tuple-element.5.returned, s32[2,128]{1,0:T(2,128)} %bitcast.15, f32[2,128]{1,0:T(2,128)} %bitcast.18), custom_call_target="tpu_custom_call" | custom-call | tf_op jit(solution)/shard_map/finish/pallas_call | solution.py:580

commit v4 on v3

--- a/solution.py
+++ b/solution.py
@@ -199,17 +199,90 @@
 
     barrier = pltpu.get_barrier_semaphore()
 
-    @pl.loop(1, n, unroll=9)
+    def greet(there):
+        pl.semaphore_signal(barrier, inc=1, device_id=there, device_id_type=MESH)
+
+    for there in (mate, 3 - mate):
+        greet({"tp": there})
+
+    @pl.loop(0, n // 2, unroll=8)
     def _(d):
-        pl.semaphore_signal(barrier, inc=1, device_id={"ep": (ep + d) % n}, device_id_type=MESH)
-
-    @pl.loop(0, n, unroll=8)
-    def _(d):
-        there = {"ep": (ep + d) % n, "tp": across}
-        pl.semaphore_signal(barrier, inc=1, device_id=there, device_id_type=MESH)
-
-    for there in (mate, 3 - mate):
-        pl.semaphore_signal(barrier, inc=1, device_id={"tp": there}, device_id_type=MESH)
+        greet({"ep": (ep + 2 * d + 1) % n})
+        greet({"ep": (ep + 2 * d) % n, "tp": across})
+
+    @pl.when(prime)
+    def _():
+        @pl.loop(1, n // 2)
+        def _(d):
+            greet({"ep": (ep + 2 * d) % n})
+
+        pl.semaphore_wait(barrier, 2 + n + n // 2 - 1)
+
+    @pl.when(jnp.logical_not(prime))
+    def _():
+        @pl.loop(0, n // 2, unroll=8)
+        def _(d):
+            greet({"ep": (ep + 2 * d + 1) % n, "tp": across})
+
+        for d in range(1, 4):
+            greet({"ep": z * 8 + (m + 2 * d) % 8})
+        for d in range(1, 8):
+            greet({"ep": ((z + d) % 8) * 8 + m})
+        pl.semaphore_wait(barrier, 2 + n + n // 2 + 10)
+
+    pieces = ((gate_hbm, g_buf), (up_hbm, u_buf), (down_hbm, d_buf))
+    sibling = {"ep": ep + other}
+
+    def put(src, i, slot, sem, where):
+        remote(src, pieces[i][1].at[slot], ws.at[sem], wr.at[3 * slot + i], where).start()
+
+    def land(i, slot):
+        wait_bytes(pieces[i][1].at[slot], wr.at[3 * slot + i])
+
+    half = d_buf.shape[1] // 2
+    halves = (pl.ds(0, half), pl.ds(half, half))
+
+    def last(src, h, sem, where):
+        remote(src, d_buf.at[3, halves[h]], ws.at[sem], wr.at[(11, 16)[h]], where).start()
+
+    def last_land(h):
+        wait_bytes(d_buf.at[3, halves[h]], wr.at[(11, 16)[h]])
+
+    def hop(i):
+        @pl.when(prime)
+        def _():
+            land(i, 2)
+            if i < 2:
+                put(pieces[i][1].at[2], i, 3, 6 + i, {"tp": mate})
+            else:
+                for h in range(2):
+                    last(d_buf.at[2, halves[h]], h, (8, 21)[h], {"tp": mate})
+            put(pieces[i][1].at[2], i, 2, 9 + i, sibling)
+
+    def share(i, slot):
+        @pl.when(prime)
+        def _():
+            land(i, slot)
+            put(pieces[i][1].at[slot], i, slot, 12 + 3 * (slot // 3) + i, sibling)
+
+    def others_land(i, slot):
+        @pl.when(jnp.logical_not(prime))
+        def _():
+            land(i, slot)
+
+    @pl.when(prime)
+    def _():
+        for i, (src, dst) in enumerate(pieces):
+            put(src, i, 1, i, {"tp": mate})
+        for i, (src, dst) in enumerate(pieces):
+            put(src, i, 0, 3 + i, sibling)
+            pltpu.make_async_copy(src, dst.at[0], wr.at[i]).start()
+
+    @pl.when(jnp.logical_not(prime))
+    def _():
+        for i, (src, dst) in enumerate(pieces):
+            put(src, i, 2, i, {"tp": across})
+
     for load in small[:2] + loads[:1]:
         load.wait()
     rows = xin[...].astype(F)
@@ -222,69 +295,22 @@
             dg(marks[128 * b : 128 * b + 128], normed, NN).reshape(16, 8, -1).astype(B)
         )
 
-    pl.semaphore_wait(barrier, 2 * n + 1)
-
-    pieces = ((gate_hbm, g_buf), (up_hbm, u_buf), (down_hbm, d_buf))
-    sibling = {"ep": ep + other}
-
-    def put(src, i, slot, sem, where):
-        remote(src, pieces[i][1].at[slot], ws.at[sem], wr.at[3 * slot + i], where).start()
-
-    def land(i, slot):
-        wait_bytes(pieces[i][1].at[slot], wr.at[3 * slot + i])
-
-    half = d_buf.shape[1] // 2
-    halves = (pl.ds(0, half), pl.ds(half, half))
-
-    def last(src, h, sem, where):
-        remote(src, d_buf.at[3, halves[h]], ws.at[sem], wr.at[(11, 16)[h]], where).start()
-
-    def last_land(h):
-        wait_bytes(d_buf.at[3, halves[h]], wr.at[(11, 16)[h]])
-
-    def hop(i):
-        @pl.when(prime)
-        def _():
-            land(i, 2)
-            if i < 2:
-                put(pieces[i][1].at[2], i, 3, 6 + i, {"tp": mate})
-            else:
-                for h in range(2):
-                    last(d_buf.at[2, halves[h]], h, (8, 21)[h], {"tp": mate})
-            put(pieces[i][1].at[2], i, 2, 9 + i, sibling)
-
-    def share(i, slot):
-        @pl.when(prime)
-        def _():
-            land(i, slot)
-            put(pieces[i][1].at[slot], i, slot, 12 + 3 * (slot // 3) + i, sibling)
-
-    def others_land(i, slot):
-        @pl.when(jnp.logical_not(prime))
-        def _():
-            land(i, slot)
-
-    @pl.when(prime)
-    def _():
-        for i, (src, dst) in enumerate(pieces):
-            put(src, i, 1, i, {"tp": mate})
-        for i, (src, dst) in enumerate(pieces):
-            put(src, i, 0, 3 + i, sibling)
-            pltpu.make_async_copy(src, dst.at[0], wr.at[i]).start()
-
-    @pl.when(jnp.logical_not(prime))
-    def _():
-        for i, (src, dst) in enumerate(pieces):
-            put(src, i, 2, i, {"tp": across})
-
     def dispatch(e):
         differ = (e % 2 + tp // 2) % 2
         there = {"ep": e + differ * (1 - 2 * (e % 2)), "tp": tp + differ * (3 - 2 * tp)}
         remote(out_buf.at[e], arr_buf.at[ep], s4.at[0], s4.at[1], there).start()
 
+    odd = jnp.where(prime, 0, 1)
+
     @pl.loop(0, n // 2)
     def _(d):
-        dispatch((ep + 2 * d + 1) % n)
+        @pl.when(d + odd > 0)
+        def _():
+            dispatch((ep + 2 * d + odd) % n)
+
+    @pl.when(prime)
+    def _():
+        pltpu.make_async_copy(out_buf.at[ep], arr_buf.at[ep], s4.at[1]).start()
 
     for load in small[2:] + loads[1:6]:
         load.wait()
@@ -314,9 +340,9 @@
     for d in range(1, 8):
         row_copy(d, m).start()
 
-    @pl.loop(1, n // 4)
+    @pl.loop(0, n // 4)
     def _(d):
-        dispatch((ep + 4 * d) % n)
+        dispatch((ep + 4 * d + 1 - odd) % n)
 
     hop(0)
     row_buf[m] = mb_buf[x]
@@ -340,17 +366,9 @@
     for d in range(1, 8):
         z_copy(d, z).start()
 
-    @pl.when(prime)
-    def _():
-        pltpu.make_async_copy(out_buf.at[ep], arr_buf.at[ep], s4.at[1]).start()
-
-    @pl.when(jnp.logical_not(prime))
-    def _():
-        dispatch(ep)
-
     @pl.loop(0, n // 4)
     def _(d):
-        dispatch((ep + 4 * d + 2) % n)
+        dispatch((ep + 4 * d + 3 - odd) % n)
 
     hop(1)
     for i in range(3):

time: 139 us -> 138 us (level)
  no operation moved by 1% of the time
where the time goes in v4:
time: 138 us; the launch traced here: 136 us
  Pallas kernels  136 us (99%)
    pallas_call x1, Pallas kernels, on_device(): pl.pallas_call(kernel, in_specs=[anywhere] * 15, out_specs=[anywhere, any...  133 us
    pallas_call x1, Pallas kernels, on_device(): pl.pallas_call(finish_kernel, in_specs=[anywhere] * 4, out_specs=[anywher...  3.12 us

profile of v4, /device:TPU:1, one launch (start us, length us, event | category | flops | bytes accessed | tf_op | source)
XLA Modules:
  0.0 136.4 jit_solution(5017690567009944812)
XLA Ops:
  0.6 132.6 %step.1 = (bf16[128,2048]{1,0:T(8,128)(2,1)}, bf16[64,8,2048]{2,1,0:T(8,128)(2,1)}) custom-call(bf16[512,512]{1,0:T(8,128)(2,1)} %rec_hbm.1, bf16[512,512]{1,0:T(8,128)(2,1)} %key_hbm.1, bf16[512,512]{1,0:T(8,128)(2,1)} %val_hbm.1, bf16[512,512]{1,0:T(8,128)(2,1)} %dec_hbm.1, bf16[512,512]{1,0:T(8,128)(2,1)} %learn_hbm.1, bf16[512,2048]{1,0:T(8,128)(2,1)} %wout_hbm.1, ...), custom_call_target="tpu_custom_call" | custom-call | tf_op jit(solution)/shard_map/step/pallas_call | solution.py:571
  133.3 3.1 %finish.1 = (bf16[128,2048]{1,0:T(8,128)(2,1)}, bf16[128,2048]{1,0:T(8,128)(2,1)}) custom-call(bf16[128,2048]{1,0:T(8,128)(2,1)} %get-tuple-element.4.mixed, bf16[64,8,2048]{2,1,0:T(8,128)(2,1)} %get-tuple-element.5.returned, s32[2,128]{1,0:T(2,128)} %bitcast.15, f32[2,128]{1,0:T(2,128)} %bitcast.18), custom_call_target="tpu_custom_call" | custom-call | tf_op jit(solution)/shard_map/finish/pallas_call | solution.py:598
